TPU v7x, 512 devices: a whole 4x8x8 slice. The times are simulated.
512 devices in a mesh: ep: 32 (over z, x), tp: 16 (over y, core).
Axes of the slice: x: 4, y: 8, z: 8, core: 2. Of those that a mesh axis runs over, the one named last changes fastest.
Arguments:
- mixer_input: bfloat16 [4096, 2048], P('ep'), may hold values from -6 to 6
- mixer_gain: float32 [2048], replicated, may hold values from 0.1 to 1.9
- outer_weight: bfloat16 [2048, 1024], P(None, 'tp'), may hold values from -0.125 to 0.125
- inner_weight: bfloat16 [2048, 1024], P(None, 'tp'), may hold values from -0.125 to 0.125
- value_weight: bfloat16 [2048, 1024], P(None, 'tp'), may hold values from -0.125 to 0.125
- conv_kernel: bfloat16 [3, 1024], P(None, 'tp'), may hold values from -3 to 3
- group_gain: float32 [1024], P('tp'), may hold values from 0.1 to 1.9
- mixer_out_weight: bfloat16 [1024, 2048], P(None, 'tp'), may hold values from -0.1875 to 0.1875
- expert_input: bfloat16 [8192, 2048], P('ep'), may hold values from -6 to 6
- expert_gain: float32 [2048], replicated, may hold values from 0.1 to 1.9
- routes: int32 [8192, 2], P('ep'), may hold values from 0 to 31, all different within a row; in each aligned block of 256 rows (0 to 255, 256 to 511, ...) at most 32 rows name the same one
- route_weight: float32 [8192, 2], P('ep'), may hold values from 0.1 to 1
- expert_gate: bfloat16 [32, 2048, 3584], P('ep', None, 'tp'), may hold values from -0.125 to 0.125
- expert_up: bfloat16 [32, 2048, 3584], P('ep', None, 'tp'), may hold values from -0.125 to 0.125
- expert_down: bfloat16 [32, 3584, 2048], P('ep', None, 'tp'), may hold values from -0.09375 to 0.09375
Outputs:
- mixed_tokens: bfloat16 [4096, 2048], P('ep', 'tp')
- expert_tokens: bfloat16 [8192, 2048], P('ep', 'tp')
Inputs may be any that keep to these rules, and one draw needn't show every extreme that they name: `routes`: each row names 2 different experts. Within the rows of one index of ep no expert is named by more than 32 rows, a bound that some block reaches of them.
All inputs are finite; a program needn't handle non-finite values.
Results may differ from a plain program's by a relative error of at most 0.014.
Values may be sent and summed in bfloat16 or wider, within the bound.
A program may use at most 64 MiB of HBM per device.

v0:
```python
import jax
import jax.numpy as jnp
from jax import lax
from jax.sharding import PartitionSpec as P

GROUP = 64
EPS = 1e-06


def from_behind(block, axis, distance):
    devices = range(lax.axis_size(axis))
    route = [(i - distance, i) for i in devices if i - distance in devices]
    return lax.ppermute(block, axis, route)


def laid_out(tiles, dim):
    tiles = jnp.moveaxis(tiles, 0, dim)
    lengths = tiles.shape
    return tiles.reshape(*lengths[:dim], lengths[dim] * lengths[dim + 1], *lengths[dim + 2 :])


def sent_to_all(value, axis):
    size = lax.axis_size(axis)
    return lax.all_to_all(
        jnp.broadcast_to(value[None], (size, *value.shape)), axis, 0, 0, tiled=True
    )


def collect(value, axis, dim):
    return laid_out(sent_to_all(value, axis), dim)


def rms_scale(values, gain):
    floats = values.astype(jnp.float32)
    scale = lax.rsqrt(jnp.mean(floats * floats, axis=-1, keepdims=True) + EPS)
    return floats * scale * gain


def per_device(
    mixer_input,
    mixer_gain,
    outer_weight,
    inner_weight,
    value_weight,
    conv_kernel,
    group_gain,
    mixer_out_weight,
    expert_input,
    expert_gain,
    routes,
    route_weight,
    expert_gate,
    expert_up,
    expert_down,
):
    mix_count = mixer_input.shape[0]
    normed_a = rms_scale(mixer_input, mixer_gain).astype(jnp.bfloat16)
    outer = jnp.dot(normed_a, outer_weight, preferred_element_type=jnp.float32).astype(jnp.bfloat16)
    inner = jnp.dot(normed_a, inner_weight, preferred_element_type=jnp.float32).astype(jnp.bfloat16)
    values = jnp.dot(normed_a, value_weight, preferred_element_type=jnp.float32).astype(
        jnp.bfloat16
    )
    product = inner.astype(jnp.float32) * values.astype(jnp.float32)
    earlier_rows = from_behind(product[mix_count - 2 :], "ep", 1)
    padded = jnp.concatenate([earlier_rows, product], axis=0)
    kernel = conv_kernel.astype(jnp.float32)
    conv_sum = (
        kernel[0] * padded[0:mix_count]
        + kernel[1] * padded[1 : mix_count + 1]
        + kernel[2] * padded[2 : mix_count + 2]
    )
    gated = outer.astype(jnp.float32) * conv_sum
    grouped = gated.reshape(mix_count, -1, GROUP)
    grouped = rms_scale(grouped, group_gain.reshape(-1, GROUP))
    grouped = grouped.reshape(mix_count, -1).astype(jnp.bfloat16)
    weight_rows = mixer_out_weight
    mixed_tokens = jnp.dot(
        collect(grouped, "tp", 1), weight_rows, preferred_element_type=jnp.float32
    ).astype(jnp.bfloat16)
    exp_count, picks_each = routes.shape
    width = expert_input.shape[1]
    experts = expert_gate.shape[0] * lax.axis_size("ep")
    capacity = 2 * picks_each * exp_count // experts
    normed_b = rms_scale(expert_input, expert_gain).astype(jnp.bfloat16)
    picks = routes.reshape(-1)
    onehot = (picks[:, None] == jnp.arange(experts, dtype=jnp.int32)[None, :]).astype(jnp.int32)
    rank = jnp.sum((jnp.cumsum(onehot, axis=0) - onehot) * onehot, axis=1)
    slot = picks * capacity + rank
    token = jnp.arange(exp_count * picks_each, dtype=jnp.int32) // picks_each
    table = jnp.zeros((experts * capacity,), jnp.int32).at[slot].set(token + 1)
    valid = table > 0
    gathered_rows = jnp.take(normed_b, jnp.maximum(table - 1, 0), axis=0)
    buffer = jnp.where(valid[:, None], gathered_rows, 0).reshape(experts, capacity, width)
    gate_weight = expert_gate[0]
    up_weight = expert_up[0]
    down_weight = expert_down[0]
    out_cols = down_weight.shape[1]
    span = width // lax.axis_size("tp")
    outgoing = lax.dynamic_slice_in_dim(buffer, lax.axis_index("tp") * span, span, 2)
    received = lax.all_to_all(outgoing, "ep", split_axis=0, concat_axis=0, tiled=True)
    sources = received.shape[0]
    count = received.shape[1]
    piece = lax.all_gather(received, "tp", axis=2, tiled=True)
    span = piece.shape[2]
    flat_piece = piece.reshape(sources * count, span)
    gate = jnp.dot(flat_piece, gate_weight, preferred_element_type=jnp.float32)
    up_value = jnp.dot(flat_piece, up_weight, preferred_element_type=jnp.float32)
    hidden = (jax.nn.silu(gate) * up_value).astype(jnp.bfloat16)
    weight_rows = down_weight
    results = jnp.dot(
        lax.all_gather(hidden, "tp", axis=1, tiled=True),
        weight_rows,
        preferred_element_type=jnp.float32,
    ).astype(jnp.bfloat16)
    returned = lax.all_to_all(
        results.reshape(sources, count, out_cols), "ep", split_axis=0, concat_axis=0, tiled=True
    )
    flat_returned = returned.reshape(experts * capacity, out_cols)
    chosen = (
        jnp.take(flat_returned, slot, axis=0)
        .astype(jnp.float32)
        .reshape(exp_count, picks_each, out_cols)
    )
    weighted = jnp.sum(chosen * route_weight[..., None], axis=1)
    expert_tokens = weighted.astype(jnp.bfloat16)
    return (mixed_tokens, expert_tokens)


def solution(mesh):
    placed = (
        P("ep", None),
        P(),
        P(None, "tp"),
        P(None, "tp"),
        P(None, "tp"),
        P(None, "tp"),
        P("tp"),
        P(None, "tp"),
        P("ep", None),
        P(),
        P("ep", None),
        P("ep", None),
        P("ep", None, "tp"),
        P("ep", None, "tp"),
        P("ep", None, "tp"),
    )
    return jax.shard_map(
        per_device,
        mesh=mesh,
        in_specs=placed,
        out_specs=(P("ep", "tp"), P("ep", "tp")),
        check_vma=False,
    )
```

profile of v0, /device:TPU:24, one launch (start us, length us, event | category | flops | bytes accessed | tf_op | source)
XLA Modules:
  0.0 200.4 jit_solution(5589004506806771158)
XLA Ops:
  7.2 0.9 copy.25
  8.4 0.7 broadcast_multiply_fusion
  9.1 1.2 reduce-window.6
  11.0 2.4 %scatter_custom_fusion = s32[1024]{0:T(1024)S(1)} fusion(s32[512]{0:T(512)S(1)} %bitcast.57, s32[512]{0:T(512)S(1)} %fusion.28, s32[]{:T(128)} %constant.74.clone.1), kind=kCustom, calls=%fused_computation.67 | custom fusion | bytes 4100 | tf_op jit(solution)/shard_map/scatter | solution.py:90
  13.6 1.5 fusion
  15.1 1.5 fusion.2
  16.7 6.0 %gather_fusion = bf16[1024,2048]{1,0:T(8,128)(2,1)} fusion(bf16[256,2048]{1,0:T(8,128)(2,1)S(1)} %fusion.2, s32[1024]{0:T(1024)S(1)} %fusion.26), kind=kCustom, calls=%fused_computation | custom fusion | bytes 8392704 | tf_op jit(solution)/shard_map/jit(_take)/gather | solution.py:92
  22.6 1.4 fusion.15
  24.0 25.9 %all_to_all.15 = bf16[32,32,128]{2,1,0:T(8,128)(2,1)} all-to-all(bf16[32,32,128]{2,1,0:T(8,128)(2,1)S(1)} %fusion.15), channel_id=1, replica_groups=mesh['ep'=32,'tp'=16] {'ep'}, dimensions={0} | all-to-all | bytes 524288 | tf_op jit(solution)/shard_map/all_to_all | solution.py:100
  50.0 45.5 %all-gather.3.cloned.1.call-done = bf16[32,32,2048]{2,1,0:T(8,128)(2,1)} async-done(((bf16[32,32,128]{2,1,0:T(8,128)(2,1)}), bf16[32,32,2048]{2,1,0:T(8,128)(2,1)}) %all-gather.3.cloned.1.call-update) | async-done | bytes 4194320 | tf_op jit(solution)/shard_map/all_gather | solution.py:103
  95.5 3.7 %fusion.13 = f32[1024,224]{0,1:T(8,128)S(1)} fusion(bf16[1024,2048]{1,0:T(8,128)(2,1)} %bitcast.59, bf16[1,2048,224]{1,2,0:T(8,128)(2,1)S(1)} %copy-done), kind=kOutput, calls=%fused_computation.26 | convolution fusion | flops 939524096 | bytes 6029312 | tf_op jit(solution)/shard_map/dot_general | solution.py:106
  99.3 2.3 %fusion.3 = bf16[1024,224]{0,1:T(8,128)(2,1)} fusion(bf16[1024,2048]{1,0:T(8,128)(2,1)S(1)} %bitcast.60, bf16[1,2048,224]{1,2,0:T(8,128)(2,1)S(1)} %copy-done.8, f32[1024,224]{0,1:T(8,128)S(1)} %fusion.13), kind=kOutput, calls=%fused_computation.11 | convolution fusion | flops 940900352 | bytes 6488064 | tf_op jit(solution)/shard_map/dot_general | solution.py:107
  102.6 3.4 %collective-permute-start = (f32[2,64]{0,1:T(8,128)S(1)}, f32[2,64]{0,1:T(8,128)S(1)}, u32[]{:S(2)}, u32[]{:S(2)}) collective-permute-start(f32[2,64]{0,1:T(8,128)S(1)} %slice.36), channel_id=1, source_target_pairs={{0,16},{16,32},{32,48},{48,64},{64,80},{80,96},{96,112},{112,128},... | collective-permute-start | bytes 1544 | tf_op jit(solution)/shard_map/ppermute | solution.py:13
  106.3 1.3 collective-permute-done
  107.6 0.4 multiply_reduce_fusion.1
  108.1 0.8 broadcast_in_dim.53
  108.9 6.2 %all-to-all-start = ((bf16[16,128,64]{1,2,0:T(8,128)(2,1)}), bf16[16,128,64]{1,2,0:T(8,128)(2,1)S(1)}, u32[]{:S(2)}, u32[]{:S(2)}) async-start(bf16[16,128,64]{1,2,0:T(8,128)(2,1)} %broadcast_in_dim.53), calls=%async_computation | async-start | bytes 524288 | tf_op jit(solution)/shard_map/all_to_all | solution.py:24
  115.0 45.4 %all-gather.5.cloned.1.call-done = bf16[1024,3584]{0,1:T(8,128)(2,1)} async-done(((bf16[1024,224]{0,1:T(8,128)(2,1)}), bf16[1024,3584]{0,1:T(8,128)(2,1)}) %all-gather.5.cloned.1.call-update) | async-done | bytes 7340048 | tf_op jit(solution)/shard_map/all_gather | solution.py:111
  160.5 5.9 %convolution_convert_fusion = bf16[1024,128]{1,0:T(8,128)(2,1)} fusion(bf16[1024,3584]{0,1:T(8,128)(2,1)} %all-gather.5.cloned.1.call-done, bf16[1,3584,128]{2,1,0:T(8,128)(2,1)S(1)} %copy-done.9), kind=kOutput, calls=%fused_computation.12 | convolution fusion | flops 939655168 | bytes 8519680 | tf_op jit(solution)/shard_map/dot_general | solution.py:110
  166.4 10.3 %all-to-all-start.2 = ((bf16[32,32,128]{2,1,0:T(8,128)(2,1)}), bf16[32,32,128]{2,1,0:T(8,128)(2,1)S(1)}, u32[]{:S(2)}, u32[]{:S(2)}) async-start(bf16[32,32,128]{2,1,0:T(8,128)(2,1)} %bitcast.13), calls=%async_computation.2 | async-start | bytes 524288 | tf_op jit(solution)/shard_map/all_to_all | solution.py:115
  177.1 0.9 convolution_convert_fusion.1
  178.0 12.1 %all-to-all-done.2 = bf16[32,32,128]{2,1,0:T(8,128)(2,1)S(1)} async-done(((bf16[32,32,128]{2,1,0:T(8,128)(2,1)}), bf16[32,32,128]{2,1,0:T(8,128)(2,1)S(1)}, u32[]{:S(2)}, u32[]{:S(2)}) %all-to-all-start.2) | async-done | bytes 262176 | tf_op jit(solution)/shard_map/all_to_all | solution.py:115
  190.1 1.3 gather_fusion.1
  191.4 2.1 %multiply_reduce_fusion = bf16[256,128]{1,0:T(8,128)(2,1)} fusion(bf16[256,2,128]{2,1,0:T(2,128)(2,1)S(1)} %bitcast.55, pred[256,2]{1,0:T(8,128)(4,1)S(1)} %copy.29, f32[256,2]{1,0:T(8,128)S(1)} %copy.31), kind=kLoop, calls=%fused_computation.30 | loop fusion | flops 229376 | bytes 199168 | tf_op jit(solution)/shard_map/reduce_sum | solution.py:124
  (64 shorter events, 3.0 us)
Async XLA Ops:
  7.2 88.3 %copy-start = (bf16[1,2048,224]{1,2,0:T(8,128)(2,1)S(1)}, bf16[1,2048,224]{1,2,0:T(8,128)(2,1)}, u32[]{:S(2)}) copy-start(bf16[1,2048,224]{1,2,0:T(8,128)(2,1)} %param.27) | copy-start | bytes 2752516
  7.2 88.3 %all-gather.3.cloned.1.call-start = ((), (), s32[]{:S(2)}) async-start(), calls=%async_computation.3 | async-start | bytes 4456448 | tf_op jit(solution)/shard_map/all_gather | solution.py:103
  22.6 76.6 %copy-start.8 = (bf16[1,2048,224]{1,2,0:T(8,128)(2,1)S(1)}, bf16[1,2048,224]{1,2,0:T(8,128)(2,1)}, u32[]{:S(2)}) copy-start(bf16[1,2048,224]{1,2,0:T(8,128)(2,1)} %param.28) | copy-start | bytes 2752516
  49.9 110.5 %all-gather.5.cloned.1.call-start = ((), (), s32[]{:S(2)}) async-start(), calls=%async_computation.4 | async-start | bytes 7798784 | tf_op jit(solution)/shard_map/all_gather | solution.py:111
  95.5 3.7 %copy-start.7 = (bf16[32,32,2048]{2,1,0:T(8,128)(2,1)S(1)}, bf16[32,32,2048]{2,1,0:T(8,128)(2,1)}, u32[]{:S(2)}) copy-start(bf16[32,32,2048]{2,1,0:T(8,128)(2,1)} %all-gather.3.cloned.1.call-done) | copy-start | bytes 12582916
  99.2 2.4 %copy-start.1 = (bf16[128,2048]{1,0:T(8,128)(2,1)S(1)}, bf16[128,2048]{1,0:T(8,128)(2,1)}, u32[]{:S(2)}) copy-start(bf16[128,2048]{1,0:T(8,128)(2,1)} %param.15) | copy-start | bytes 1572868
  99.2 2.6 %copy-start.10 = (bf16[2048,64]{0,1:T(8,128)(2,1)S(1)}, bf16[2048,64]{0,1:T(8,128)(2,1)}, u32[]{:S(2)}) copy-start(bf16[2048,64]{0,1:T(8,128)(2,1)} %param.18) | copy-start | bytes 786436
  99.3 2.6 %copy-start.13 = (f32[2048]{0:T(1024)S(1)}, f32[2048]{0:T(1024)}, u32[]{:S(2)}) copy-start(f32[2048]{0:T(1024)} %param.16) | copy-start | bytes 24580
  99.3 2.9 %copy-start.11 = (bf16[2048,64]{0,1:T(8,128)(2,1)S(1)}, bf16[2048,64]{0,1:T(8,128)(2,1)}, u32[]{:S(2)}) copy-start(bf16[2048,64]{0,1:T(8,128)(2,1)} %param.19) | copy-start | bytes 786436
  99.3 6.8 %copy-start.5 = (bf16[3,64]{1,0:T(4,128)(2,1)S(1)}, bf16[3,64]{1,0:T(4,128)(2,1)}, u32[]{:S(2)}) copy-start(bf16[3,64]{1,0:T(4,128)(2,1)} %param.20) | copy-start | bytes 1156
  99.3 8.3 %copy-start.12 = (bf16[2048,64]{0,1:T(8,128)(2,1)S(1)}, bf16[2048,64]{0,1:T(8,128)(2,1)}, u32[]{:S(2)}) copy-start(bf16[2048,64]{0,1:T(8,128)(2,1)} %param.17) | copy-start | bytes 786436
  101.6 6.5 %copy-start.6 = (f32[64]{0:T(128)S(1)}, f32[64]{0:T(128)}, u32[]{:S(2)}) copy-start(f32[64]{0:T(128)} %param.21) | copy-start | bytes 772
  101.6 58.9 %copy-start.9 = (bf16[1,3584,128]{2,1,0:T(8,128)(2,1)S(1)}, bf16[1,3584,128]{2,1,0:T(8,128)(2,1)}, u32[]{:S(2)}) copy-start(bf16[1,3584,128]{2,1,0:T(8,128)(2,1)} %param.29) | copy-start | bytes 2752516
  102.6 5.0 %collective-permute-start = (f32[2,64]{0,1:T(8,128)S(1)}, f32[2,64]{0,1:T(8,128)S(1)}, u32[]{:S(2)}, u32[]{:S(2)}) collective-permute-start(f32[2,64]{0,1:T(8,128)S(1)} %slice.36), channel_id=1, source_target_pairs={{0,16},{16,32},{32,48},{48,64},{64,80},{80,96},{96,112},{112,128},... | collective-permute-start | bytes 1544 | tf_op jit(solution)/shard_map/ppermute | solution.py:13
  108.9 57.5 %all-to-all-start = ((bf16[16,128,64]{1,2,0:T(8,128)(2,1)}), bf16[16,128,64]{1,2,0:T(8,128)(2,1)S(1)}, u32[]{:S(2)}, u32[]{:S(2)}) async-start(bf16[16,128,64]{1,2,0:T(8,128)(2,1)} %broadcast_in_dim.53), calls=%async_computation | async-start | bytes 524288 | tf_op jit(solution)/shard_map/all_to_all | solution.py:24
  115.0 61.7 %copy-start.3 = (s32[256,2]{0,1:T(2,128)S(1)}, s32[256,2]{0,1:T(2,128)}, u32[]{:S(2)}) copy-start(s32[256,2]{0,1:T(2,128)} %param.25) | copy-start | bytes 6148
  115.0 61.9 %copy-start.4 = (f32[256,2]{0,1:T(2,128)S(1)}, f32[256,2]{0,1:T(2,128)}, u32[]{:S(2)}) copy-start(f32[256,2]{0,1:T(2,128)} %param.26) | copy-start | bytes 6148
  115.0 62.1 %copy-start.2 = (bf16[1024,128]{1,0:T(8,128)(2,1)S(1)}, bf16[1024,128]{1,0:T(8,128)(2,1)}, u32[]{:S(2)}) copy-start(bf16[1024,128]{1,0:T(8,128)(2,1)} %param.22) | copy-start | bytes 786436
  166.4 23.7 %all-to-all-start.2 = ((bf16[32,32,128]{2,1,0:T(8,128)(2,1)}), bf16[32,32,128]{2,1,0:T(8,128)(2,1)S(1)}, u32[]{:S(2)}, u32[]{:S(2)}) async-start(bf16[32,32,128]{2,1,0:T(8,128)(2,1)} %bitcast.13), calls=%async_computation.2 | async-start | bytes 524288 | tf_op jit(solution)/shard_map/all_to_all | solution.py:115
Sparse Core Ops, SparseCore 0:
  50.1 45.3 all-gather.2
  101.7 58.7 all-gather.4
where the time goes:
time: 201 us; the launch traced here: 200 us
  waiting for transfers between devices  104 us (52%)
  blocking collectives  25.9 us (13%)
  starting transfers between devices  19.9 us (10%)
  between operations  14.4 us (7%)
  matrix products  13.9 us (7%)
  local copies, waits for them, and re-layouts  13 us (6%)
  other arithmetic  8.83 us (4%)
    all_gather x1, waiting for transfers between devices, per_device(): piece = lax.all_gather(received, 'tp', axis=2, tiled=True)  45.5 us
    all_gather x1, waiting for transfers between devices, per_device(): lax.all_gather(hidden, 'tp', axis=1, tiled=True)  45.4 us
    all_to_all x1, blocking collectives, per_device(): lax.all_to_all(outgoing, 'ep', split_axis=0, concat_axis=0, tiled=True)  25.9 us
    all_to_all x1, waiting for transfers between devices, per_device(): lax.all_to_all(results.reshape(sources, count, out_cols), 'ep', split_axi...  12.1 us
    all_to_all x1, starting transfers between devices, per_device(): lax.all_to_all(results.reshape(sources, count, out_cols), 'ep', split_axi...  10.3 us
    all_to_all x1, starting transfers between devices, sent_to_all(): lax.all_to_all(jnp.broadcast_to(value[None], (size, *value.shape)), axis,...  6.16 us
    gather x1, local copies, waits for them, and re-layouts, per_device(): gathered_rows = jnp.take(normed_b, jnp.maximum(table - 1, 0), axis=0)  5.98 us
    dot_general x1, matrix products, per_device(): jnp.dot(lax.all_gather(hidden, 'tp', axis=1, tiled=True), weight_rows, pr...  5.92 us
  transfers between devices with their start and end apart: 5, of which 4 were waited for; matrix products, arithmetic and copies ran while one was open for 5% of the time, Pallas kernels for 0%

commit v1 on v0

--- a/solution.py
+++ b/solution.py
@@ -108,7 +108,9 @@
     hidden = (jax.nn.silu(gate) * up_value).astype(jnp.bfloat16)
     weight_rows = down_weight
     results = jnp.dot(
-        lax.all_gather(hidden, "tp", axis=1, tiled=True),
+        jnp.concatenate(
+            lax.all_to_all(jnp.stack([hidden] * lax.axis_size("tp")), "tp", 0, 0), axis=1
+        ),
         weight_rows,
         preferred_element_type=jnp.float32,
     ).astype(jnp.bfloat16)

time: 201 us -> 324 us (1.61)
  the two profiles are of different devices: /device:TPU:24 before, /device:TPU:1 now
where the time goes in v1:
time: 324 us
  waiting for transfers between devices  224 us (69%)
  blocking collectives  24.9 us (8%)
  starting transfers between devices  21.4 us (7%)
  local copies, waits for them, and re-layouts  17 us (5%)
  between operations  14.4 us (4%)
  matrix products  13.2 us (4%)
  other arithmetic  8.83 us (3%)
    all_to_all x1, waiting for transfers between devices, per_device(): lax.all_to_all(jnp.stack([hidden] * lax.axis_size('tp')), 'tp', 0, 0)  156 us
    all_gather x1, waiting for transfers between devices, per_device(): piece = lax.all_gather(received, 'tp', axis=2, tiled=True)  50.3 us
    all_to_all x1, blocking collectives, per_device(): lax.all_to_all(outgoing, 'ep', split_axis=0, concat_axis=0, tiled=True)  24.9 us
    all_to_all x1, waiting for transfers between devices, per_device(): lax.all_to_all(results.reshape(sources, count, out_cols), 'ep', split_axi...  11.1 us
    all_to_all x1, starting transfers between devices, per_device(): lax.all_to_all(results.reshape(sources, count, out_cols), 'ep', split_axi...  8.95 us
  transfers between devices with their start and end apart: 5, of which 5 were waited for; matrix products, arithmetic and copies ran while one was open for 3% of the time, Pallas kernels for 0%

profile of v1, /device:TPU:1, one launch (start us, length us, event | category | flops | bytes accessed | tf_op | source)
XLA Modules:
  0.0 323.8 jit_solution(12772069146382159846)
XLA Ops:
  7.2 0.9 copy.26
  9.1 1.2 reduce-window.6
  11.0 2.4 scatter_custom_fusion
  13.6 1.5 fusion
  15.1 1.5 fusion.2
  16.7 6.0 %gather_fusion = bf16[1024,2048]{1,0:T(8,128)(2,1)} fusion(bf16[256,2048]{1,0:T(8,128)(2,1)S(1)} %fusion.2, s32[1024]{0:T(1024)S(1)} %fusion.26), kind=kCustom, calls=%fused_computation | custom fusion | bytes 8392704 | tf_op jit(solution)/shard_map/jit(_take)/gather | solution.py:92
  22.6 1.4 fusion.15
  24.0 24.9 %all_to_all.20 = bf16[32,32,128]{2,1,0:T(8,128)(2,1)} all-to-all(bf16[32,32,128]{2,1,0:T(8,128)(2,1)S(1)} %fusion.15), channel_id=1, replica_groups=mesh['ep'=32,'tp'=16] {'ep'}, dimensions={0} | all-to-all | bytes 524288 | tf_op jit(solution)/shard_map/all_to_all | solution.py:100
  49.0 50.3 %all-gather.2.cloned.1.call-done = bf16[32,32,2048]{2,1,0:T(8,128)(2,1)} async-done(((bf16[32,32,128]{2,1,0:T(8,128)(2,1)}), bf16[32,32,2048]{2,1,0:T(8,128)(2,1)}) %all-gather.2.cloned.1.call-update) | async-done | bytes 4194320 | tf_op jit(solution)/shard_map/all_gather | solution.py:103
  99.3 3.7 %fusion.13 = f32[1024,224]{0,1:T(8,128)S(1)} fusion(bf16[1024,2048]{1,0:T(8,128)(2,1)} %bitcast.62, bf16[1,2048,224]{1,2,0:T(8,128)(2,1)S(1)} %copy-done), kind=kOutput, calls=%fused_computation.26 | convolution fusion | flops 939524096 | bytes 6029312 | tf_op jit(solution)/shard_map/dot_general | solution.py:106
  103.1 1.5 fusion.3
  104.6 4.0 %stack.2 = bf16[16,1024,224]{1,2,0:T(8,128)(2,1)} broadcast(bf16[1024,224]{0,1:T(8,128)(2,1)S(1)} %fusion.3), dimensions={1,2} | broadcast | bytes 7798784 | tf_op jit(solution)/shard_map/stack | solution.py:112
  108.6 4.8 %all-to-all-start.2 = ((bf16[16,1024,224]{1,2,0:T(8,128)(2,1)}), bf16[16,1024,224]{1,2,0:T(8,128)(2,1)}, u32[]{:S(2)}, u32[]{:S(2)}) async-start(bf16[16,1024,224]{1,2,0:T(8,128)(2,1)} %stack.2), calls=%async_computation.2 | async-start | bytes 14680064 | tf_op jit(solution)/shard_map/all_to_all | solution.py:112
  114.5 2.1 collective-permute-start
  116.9 0.8 collective-permute-done
  118.1 156.3 %all-to-all-done.2 = bf16[16,1024,224]{1,2,0:T(8,128)(2,1)} async-done(((bf16[16,1024,224]{1,2,0:T(8,128)(2,1)}), bf16[16,1024,224]{1,2,0:T(8,128)(2,1)}, u32[]{:S(2)}, u32[]{:S(2)}) %all-to-all-start.2) | async-done | bytes 7340064 | tf_op jit(solution)/shard_map/all_to_all | solution.py:112
  275.2 5.5 %all-to-all-start = ((bf16[16,128,64]{1,2,0:T(8,128)(2,1)}), bf16[16,128,64]{1,2,0:T(8,128)(2,1)S(1)}, u32[]{:S(2)}, u32[]{:S(2)}) async-start(bf16[16,128,64]{1,2,0:T(8,128)(2,1)} %broadcast_in_dim.53), calls=%async_computation | async-start | bytes 524288 | tf_op jit(solution)/shard_map/all_to_all | solution.py:24
  280.7 6.0 %convolution_convert_fusion = bf16[1024,128]{1,0:T(8,128)(2,1)} fusion(bf16[1024,3584]{0,1:T(8,128)(2,1)} %bitcast.13, bf16[1,3584,128]{2,1,0:T(8,128)(2,1)S(1)} %copy-done.9), kind=kOutput, calls=%fused_computation.12 | convolution fusion | flops 939655168 | bytes 8519680 | tf_op jit(solution)/shard_map/dot_general | solution.py:110
  286.7 5.6 %all-to-all-done = bf16[16,128,64]{1,2,0:T(8,128)(2,1)S(1)} async-done(((bf16[16,128,64]{1,2,0:T(8,128)(2,1)}), bf16[16,128,64]{1,2,0:T(8,128)(2,1)S(1)}, u32[]{:S(2)}, u32[]{:S(2)}) %all-to-all-start) | async-done | bytes 262176 | tf_op jit(solution)/shard_map/all_to_all | solution.py:24
  292.2 8.9 %all-to-all-start.3 = ((bf16[32,32,128]{2,1,0:T(8,128)(2,1)}), bf16[32,32,128]{2,1,0:T(8,128)(2,1)S(1)}, u32[]{:S(2)}, u32[]{:S(2)}) async-start(bf16[32,32,128]{2,1,0:T(8,128)(2,1)} %bitcast.15), calls=%async_computation.3 | async-start | bytes 524288 | tf_op jit(solution)/shard_map/all_to_all | solution.py:117
  301.6 0.9 convolution_convert_fusion.1
  302.5 11.1 %all-to-all-done.3 = bf16[32,32,128]{2,1,0:T(8,128)(2,1)S(1)} async-done(((bf16[32,32,128]{2,1,0:T(8,128)(2,1)}), bf16[32,32,128]{2,1,0:T(8,128)(2,1)S(1)}, u32[]{:S(2)}, u32[]{:S(2)}) %all-to-all-start.3) | async-done | bytes 262176 | tf_op jit(solution)/shard_map/all_to_all | solution.py:117
  313.5 1.3 gather_fusion.1
  314.9 2.1 multiply_reduce_fusion
  (64 shorter events, 4.7 us)
Async XLA Ops:
  7.2 92.1 %copy-start = (bf16[1,2048,224]{1,2,0:T(8,128)(2,1)S(1)}, bf16[1,2048,224]{1,2,0:T(8,128)(2,1)}, u32[]{:S(2)}) copy-start(bf16[1,2048,224]{1,2,0:T(8,128)(2,1)} %param.27) | copy-start | bytes 2752516
  7.2 92.1 %all-gather.2.cloned.1.call-start = ((), (), s32[]{:S(2)}) async-start(), calls=%async_computation.4 | async-start | bytes 4456448 | tf_op jit(solution)/shard_map/all_gather | solution.py:103
  22.6 80.4 %copy-start.8 = (bf16[1,2048,224]{1,2,0:T(8,128)(2,1)S(1)}, bf16[1,2048,224]{1,2,0:T(8,128)(2,1)}, u32[]{:S(2)}) copy-start(bf16[1,2048,224]{1,2,0:T(8,128)(2,1)} %param.28) | copy-start | bytes 2752516
  99.3 3.8 %copy-start.7 = (bf16[32,32,2048]{2,1,0:T(8,128)(2,1)S(1)}, bf16[32,32,2048]{2,1,0:T(8,128)(2,1)}, u32[]{:S(2)}) copy-start(bf16[32,32,2048]{2,1,0:T(8,128)(2,1)} %all-gather.2.cloned.1.call-done) | copy-start | bytes 12582916
  108.5 4.9 %copy-start.1 = (bf16[128,2048]{1,0:T(8,128)(2,1)S(1)}, bf16[128,2048]{1,0:T(8,128)(2,1)}, u32[]{:S(2)}) copy-start(bf16[128,2048]{1,0:T(8,128)(2,1)} %param.15) | copy-start | bytes 1572868
  108.5 5.1 %copy-start.10 = (bf16[2048,64]{0,1:T(8,128)(2,1)S(1)}, bf16[2048,64]{0,1:T(8,128)(2,1)}, u32[]{:S(2)}) copy-start(bf16[2048,64]{0,1:T(8,128)(2,1)} %param.18) | copy-start | bytes 786436
  108.5 5.1 %copy-start.13 = (f32[2048]{0:T(1024)S(1)}, f32[2048]{0:T(1024)}, u32[]{:S(2)}) copy-start(f32[2048]{0:T(1024)} %param.16) | copy-start | bytes 24580
  108.6 5.5 %copy-start.11 = (bf16[2048,64]{0,1:T(8,128)(2,1)S(1)}, bf16[2048,64]{0,1:T(8,128)(2,1)}, u32[]{:S(2)}) copy-start(bf16[2048,64]{0,1:T(8,128)(2,1)} %param.19) | copy-start | bytes 786436
  108.6 8.1 %copy-start.5 = (bf16[3,64]{1,0:T(4,128)(2,1)S(1)}, bf16[3,64]{1,0:T(4,128)(2,1)}, u32[]{:S(2)}) copy-start(bf16[3,64]{1,0:T(4,128)(2,1)} %param.20) | copy-start | bytes 1156
  108.6 9.1 %copy-start.12 = (bf16[2048,64]{0,1:T(8,128)(2,1)S(1)}, bf16[2048,64]{0,1:T(8,128)(2,1)}, u32[]{:S(2)}) copy-start(bf16[2048,64]{0,1:T(8,128)(2,1)} %param.17) | copy-start | bytes 786436
  108.6 165.8 %all-to-all-start.2 = ((bf16[16,1024,224]{1,2,0:T(8,128)(2,1)}), bf16[16,1024,224]{1,2,0:T(8,128)(2,1)}, u32[]{:S(2)}, u32[]{:S(2)}) async-start(bf16[16,1024,224]{1,2,0:T(8,128)(2,1)} %stack.2), calls=%async_computation.2 | async-start | bytes 14680064 | tf_op jit(solution)/shard_map/all_to_all | solution.py:112
  113.4 4.6 %copy-start.6 = (f32[64]{0:T(128)S(1)}, f32[64]{0:T(128)}, u32[]{:S(2)}) copy-start(f32[64]{0:T(128)} %param.21) | copy-start | bytes 772
  113.4 167.2 %copy-start.9 = (bf16[1,3584,128]{2,1,0:T(8,128)(2,1)S(1)}, bf16[1,3584,128]{2,1,0:T(8,128)(2,1)}, u32[]{:S(2)}) copy-start(bf16[1,3584,128]{2,1,0:T(8,128)(2,1)} %param.29) | copy-start | bytes 2752516
  114.5 3.1 collective-permute-start
  275.2 17.1 %all-to-all-start = ((bf16[16,128,64]{1,2,0:T(8,128)(2,1)}), bf16[16,128,64]{1,2,0:T(8,128)(2,1)S(1)}, u32[]{:S(2)}, u32[]{:S(2)}) async-start(bf16[16,128,64]{1,2,0:T(8,128)(2,1)} %broadcast_in_dim.53), calls=%async_computation | async-start | bytes 524288 | tf_op jit(solution)/shard_map/all_to_all | solution.py:24
  280.7 20.5 %copy-start.3 = (s32[256,2]{0,1:T(2,128)S(1)}, s32[256,2]{0,1:T(2,128)}, u32[]{:S(2)}) copy-start(s32[256,2]{0,1:T(2,128)} %param.25) | copy-start | bytes 6148
  280.7 20.7 %copy-start.4 = (f32[256,2]{0,1:T(2,128)S(1)}, f32[256,2]{0,1:T(2,128)}, u32[]{:S(2)}) copy-start(f32[256,2]{0,1:T(2,128)} %param.26) | copy-start | bytes 6148
  280.7 20.9 %copy-start.2 = (bf16[1024,128]{1,0:T(8,128)(2,1)S(1)}, bf16[1024,128]{1,0:T(8,128)(2,1)}, u32[]{:S(2)}) copy-start(bf16[1024,128]{1,0:T(8,128)(2,1)} %param.22) | copy-start | bytes 786436
  292.2 21.3 %all-to-all-start.3 = ((bf16[32,32,128]{2,1,0:T(8,128)(2,1)}), bf16[32,32,128]{2,1,0:T(8,128)(2,1)S(1)}, u32[]{:S(2)}, u32[]{:S(2)}) async-start(bf16[32,32,128]{2,1,0:T(8,128)(2,1)} %bitcast.15), calls=%async_computation.3 | async-start | bytes 524288 | tf_op jit(solution)/shard_map/all_to_all | solution.py:117
Sparse Core Ops, SparseCore 0:
  49.1 50.1 all-gather.1
